TPU v7x, 32 devices: a whole 2x2x4 slice. The times are simulated.
32 devices in a mesh: fs: 4 (over z), rep: 4 (over y, x), tp: 2 (over core).
Axes of the slice: x: 2, y: 2, z: 4, core: 2. Of those that a mesh axis runs over, the one named last changes fastest.
Arguments:
- input_act: bfloat16 [12288, 2048], P(('fs', 'rep')), may hold values from -6 to 6
- query_cot: bfloat16 [12288, 1024], P(('fs', 'rep'), 'tp'), may hold values from -6 to 6
- out_cot: bfloat16 [12288, 2048], P(('fs', 'rep')), may hold values from -6 to 6
- attn_out: bfloat16 [12288, 1024], P(('fs', 'rep'), 'tp'), may hold values from -6 to 6
- query_w: float32 [2048, 1024], P('fs', 'tp'), may hold values from -0.125 to 0.125
- out_w: float32 [1024, 2048], P('tp', 'fs'), may hold values from -0.1875 to 0.1875
- query_factor: bfloat16 [2048, 512], P('fs'), may hold values from -0.125 to 0.125
- out_factor: bfloat16 [2048, 512], P('fs'), may hold values from -0.125 to 0.125
- first_q: float32 [512, 1024], P('fs', 'tp'), may hold values from -6 to 6
- second_q: float32 [512, 1024], P('fs', 'tp'), may hold values from 0.075 to 120
- first_o: float32 [512, 1024], P('fs', 'tp'), may hold values from -6 to 6
- second_o: float32 [512, 1024], P('fs', 'tp'), may hold values from 0.075 to 120
Outputs:
- new_query_w: float32 [2048, 1024], P('fs', 'tp')
- new_out_w: float32 [1024, 2048], P('tp', 'fs')
- query_step: float32 [2048, 1024], P('fs', 'tp')
- out_step: float32 [1024, 2048], P('tp', 'fs')
- new_first_q: float32 [512, 1024], P('fs', 'tp')
- new_second_q: float32 [512, 1024], P('fs', 'tp')
- new_first_o: float32 [512, 1024], P('fs', 'tp')
- new_second_o: float32 [512, 1024], P('fs', 'tp')
- query_copy: bfloat16 [2048, 1024], P(None, 'tp')
- out_copy: bfloat16 [1024, 2048], P('tp')
All inputs are finite; a program needn't handle non-finite values.
Results may differ from a plain program's by a relative error of at most 0.0085.
Values may be sent and summed in bfloat16 or wider, within the bound.
A program may use at most 64 MiB of HBM per device.

v0:
```python
import math

import jax
import jax.numpy as jnp
from jax import lax
from jax.sharding import PartitionSpec as P

RANK = 512
HQ = 1024


def contract_rows(left_side, right_side):
    return lax.dot_general(
        left_side, right_side, (((0,), (0,)), ((), ())), preferred_element_type=jnp.float32
    )


def contract_exact(left_side, right_side):
    return lax.dot_general(
        left_side.astype(jnp.float32),
        right_side,
        (((0,), (0,)), ((), ())),
        precision=lax.Precision.HIGHEST,
        preferred_element_type=jnp.float32,
    )


def exact_dot(left_side, right_side):
    return jnp.dot(
        left_side, right_side, precision=lax.Precision.HIGHEST, preferred_element_type=jnp.float32
    )


def body(
    input_act,
    query_cot,
    out_cot,
    attn_out,
    query_w,
    out_w,
    query_factor,
    out_factor,
    first_q,
    second_q,
    first_o,
    second_o,
):
    heads_local = query_cot.shape[1]
    token_total = input_act.shape[0] * lax.axis_size("fs") * lax.axis_size("rep")
    scale_tokens = 1.0 / math.sqrt(token_total)
    gradient = lax.psum_scatter(
        jnp.concatenate(
            [contract_rows(input_act, query_cot), contract_rows(out_cot, attn_out)], axis=1
        ).astype(jnp.bfloat16),
        "fs",
        scatter_dimension=0,
        tiled=True,
    ).astype(jnp.float32)
    partial_value = jnp.concatenate(
        [
            contract_exact(query_factor, gradient[:, :heads_local]),
            contract_exact(out_factor, gradient[:, heads_local:]),
        ],
        axis=1,
    )
    projected = lax.psum_scatter(
        partial_value.astype(jnp.bfloat16), "fs", scatter_dimension=0, tiled=True
    ).astype(jnp.float32)
    projected = lax.psum(projected.astype(jnp.bfloat16), "rep").astype(jnp.float32) * scale_tokens
    proj_q = projected[:, :heads_local]
    proj_o = projected[:, heads_local:]
    new_first_q = 0.8 * first_q + 0.2 * proj_q
    new_second_q = 0.9 * second_q + 0.1 * proj_q * proj_q
    new_first_o = 0.8 * first_o + 0.2 * proj_o
    new_second_o = 0.9 * second_o + 0.1 * proj_o * proj_o
    dir_q = new_first_q / jnp.sqrt(new_second_q)
    dir_o = new_first_o / jnp.sqrt(new_second_o)
    local_squares = jnp.sum(dir_q * dir_q) + jnp.sum(dir_o * dir_o)
    total_squares = lax.psum(local_squares, ("fs", "tp"))
    norm_scale = jnp.sqrt(total_squares / (2 * RANK * HQ) + 1e-06)
    whole_dir_q, whole_dir_o = (
        lax.all_gather(dir_q, "fs", axis=0, tiled=True),
        lax.all_gather(dir_o, "fs", axis=0, tiled=True),
    )
    query_step = exact_dot(query_factor.astype(jnp.float32), whole_dir_q) / norm_scale
    out_step = (exact_dot(out_factor.astype(jnp.float32), whole_dir_o) / norm_scale).T
    new_query_w = query_w - 0.01 * query_step
    new_out_w = out_w - 0.01 * out_step
    query_copy = lax.all_gather(new_query_w.astype(jnp.bfloat16), "fs", axis=0, tiled=True)
    out_copy = lax.all_gather(new_out_w.astype(jnp.bfloat16), "fs", axis=1, tiled=True)
    return (
        new_query_w,
        new_out_w,
        query_step,
        out_step,
        new_first_q,
        new_second_q,
        new_first_o,
        new_second_o,
        query_copy,
        out_copy,
    )


def solution(mesh):
    return jax.shard_map(
        body,
        mesh=mesh,
        in_specs=(
            P(("fs", "rep"), None),
            P(("fs", "rep"), "tp"),
            P(("fs", "rep"), None),
            P(("fs", "rep"), "tp"),
            P("fs", "tp"),
            P("tp", "fs"),
            P("fs", None),
            P("fs", None),
            P("fs", "tp"),
            P("fs", "tp"),
            P("fs", "tp"),
            P("fs", "tp"),
        ),
        out_specs=(
            P("fs", "tp"),
            P("tp", "fs"),
            P("fs", "tp"),
            P("tp", "fs"),
            P("fs", "tp"),
            P("fs", "tp"),
            P("fs", "tp"),
            P("fs", "tp"),
            P(None, "tp"),
            P("tp", None),
        ),
        check_vma=False,
    )
```

profile of v0, /device:TPU:9, one launch (start us, length us, event | category | flops | bytes accessed | tf_op | source)
XLA Modules:
  0.0 340.0 jit_solution(11248011831809214401)
XLA Ops:
  7.2 1.8 copy-done
  9.1 3.1 convolution_convert_fusion.1
  12.2 1.9 convolution_convert_fusion
  14.1 2.5 pad_maximum_fusion
  16.7 78.0 %reduce-scatter.5.cloned.1.call-done = bf16[512,1024]{0,1:T(8,128)(2,1)} async-done(((bf16[2048,1024]{0,1:T(8,128)(2,1)}), bf16[512,1024]{0,1:T(8,128)(2,1)}) %reduce-scatter.5.cloned.1.call-update) | async-done | bytes 1048592 | tf_op jit(solution)/shard_map/reduce_scatter | solution.py:51
  96.4 1.6 fusion.1
  99.1 2.3 copy.59
  101.4 25.5 %reduce-scatter.7.cloned.1.call-done = bf16[128,1024]{1,0:T(8,128)(2,1)} async-done(((bf16[512,1024]{1,0:T(8,128)(2,1)}), bf16[128,1024]{1,0:T(8,128)(2,1)}) %reduce-scatter.7.cloned.1.call-update) | async-done | bytes 262160
  126.9 1.8 copy.60
  129.6 1.8 copy.41
  131.4 1.8 copy.42
  133.2 1.8 copy.43
  135.0 39.0 %all-reduce.2.cloned.1.call-done = bf16[128,1024]{0,1:T(8,128)(2,1)} async-done(((bf16[128,1024]{0,1:T(8,128)(2,1)}), bf16[128,1024]{0,1:T(8,128)(2,1)}) %all-reduce.2.cloned.1.call-update) | async-done | bytes 262160 | tf_op jit(solution)/shard_map/psum | solution.py:69
  175.0 2.9 multiply_reduce_fusion
  179.8 2.5 copy.45
  182.4 12.8 %psum.15 = f32[]{:T(128)} all-reduce(f32[]{:T(128)S(6)} %add.30), channel_id=1, replica_groups=mesh['fs'=4,'rep'=4,'tp'=2] {'fs','tp'}, use_global_device_ids=true, to_apply=%region_5.0 | all-reduce | flops 1 | bytes 8 | tf_op jit(solution)/shard_map/psum | solution.py:79
  195.9 9.4 %all-gather.5.cloned.1.call-done = f32[512,512]{0,1:T(8,128)} async-done(((f32[128,512]{0,1:T(8,128)}), f32[512,512]{0,1:T(8,128)}) %all-gather.5.cloned.1.call-update) | async-done | bytes 1048592 | tf_op jit(solution)/shard_map/all_gather | solution.py:82
  205.3 4.2 %fusion.8 = (bf16[512,512]{0,1:T(8,128)(2,1)}, f32[512,512]{0,1:T(8,128)}, f32[512,512]{0,1:T(8,128)}) fusion(f32[512,512]{0,1:T(8,128)} %copy.45, f32[]{:T(128)S(6)} %sqrt.11, f32[512,512]{0,1:T(8,128)} %all-gather.5.cloned.1.call-done, bf16[512,512]{1,0:T(8,128)(2,1)} %param.18), kind=kOutput, calls=%fused_computation.27 | convolution fusion | flops 1611661312 | bytes 5242884 | tf_op jit(solution)/shard_map/dot_general | solution.py:29
  209.6 2.5 copy.47
  212.2 23.5 %all-gather.7.cloned.1.call-done = f32[512,512]{0,1:T(8,128)} async-done(((f32[128,512]{0,1:T(8,128)}), f32[512,512]{0,1:T(8,128)}) %all-gather.7.cloned.1.call-update) | async-done | bytes 1048592 | tf_op jit(solution)/shard_map/all_gather | solution.py:83
  235.6 4.3 %fusion.7 = (bf16[512,512]{0,1:T(8,128)(2,1)}, f32[512,512]{0,1:T(8,128)}, f32[512,512]{0,1:T(8,128)}) fusion(f32[512,512]{0,1:T(8,128)} %copy.47, f32[]{:T(128)S(6)} %sqrt.11, f32[512,512]{0,1:T(8,128)} %all-gather.7.cloned.1.call-done, bf16[512,512]{1,0:T(8,128)(2,1)} %param.19), kind=kOutput, calls=%fused_computation.26 | convolution fusion | flops 1611661312 | bytes 5242884 | tf_op jit(solution)/shard_map/dot_general | solution.py:29
  239.9 1.8 copy.55
  241.7 1.8 copy.54
  243.5 1.8 copy.53
  246.1 2.6 copy.49
  248.7 2.5 copy.51
  251.3 2.5 copy.48
  253.8 2.5 copy.50
  256.3 26.8 %all-gather.9.cloned.1.call-done = bf16[2048,512]{0,1:T(8,128)(2,1)} async-done(((bf16[512,512]{0,1:T(8,128)(2,1)}), bf16[2048,512]{0,1:T(8,128)(2,1)}) %all-gather.9.cloned.1.call-update) | async-done | bytes 2097168 | tf_op jit(solution)/shard_map/all_gather | solution.py:89
  283.1 3.9 %copy.56 = bf16[2048,512]{1,0:T(8,128)(2,1)} copy(bf16[2048,512]{0,1:T(8,128)(2,1)} %all-gather.9.cloned.1.call-done) | data formatting | bytes 4194304
  287.1 42.1 %all-gather.11.cloned.1.call-done = bf16[512,2048]{0,1:T(8,128)(2,1)} async-done(((bf16[512,512]{0,1:T(8,128)(2,1)}), bf16[512,2048]{0,1:T(8,128)(2,1)}) %all-gather.11.cloned.1.call-update) | async-done | bytes 2097168 | tf_op jit(solution)/shard_map/all_gather | solution.py:90
  329.2 3.9 %copy.57 = bf16[512,2048]{1,0:T(8,128)(2,1)} copy(bf16[512,2048]{0,1:T(8,128)(2,1)} %all-gather.11.cloned.1.call-done) | data formatting | bytes 4194304
  (26 shorter events, 6.3 us)
Async XLA Ops:
  7.2 1.9 copy-start
  7.2 87.5 %reduce-scatter.5.cloned.1.call-start = ((), (), s32[]{:S(2)}) async-start(), calls=%async_computation.2 | async-start | bytes 5242880 | tf_op jit(solution)/shard_map/reduce_scatter | solution.py:51
  9.1 3.1 copy-start.2
  9.1 3.1 copy-start.3
  16.7 110.2 %reduce-scatter.7.cloned.1.call-start = ((), (), s32[]{:S(2)}) async-start(), calls=%async_computation.8 | async-start | bytes 1310720
  98.0 30.8 %copy-start.1 = (f32[128,512]{1,0:T(8,128)S(1)}, f32[128,512]{1,0:T(8,128)}, u32[]{:S(2)}) copy-start(f32[128,512]{1,0:T(8,128)} %param.20) | copy-start | bytes 786436
  101.4 72.6 %all-reduce.2.cloned.1.call-start = ((), (), s32[]{:S(2)}) async-start(), calls=%async_computation.3 | async-start | bytes 524288 | tf_op jit(solution)/shard_map/psum | solution.py:69
  128.7 76.6 %all-gather.5.cloned.1.call-start = ((), (), s32[]{:S(2)}) async-start(), calls=%async_computation.4 | async-start | bytes 1310720 | tf_op jit(solution)/shard_map/all_gather | solution.py:82
  177.9 57.7 %all-gather.7.cloned.1.call-start = ((), (), s32[]{:S(2)}) async-start(), calls=%async_computation.5 | async-start | bytes 1310720 | tf_op jit(solution)/shard_map/all_gather | solution.py:83
  178.5 104.7 %all-gather.9.cloned.1.call-start = ((), (), s32[]{:S(2)}) async-start(), calls=%async_computation.6 | async-start | bytes 2621440 | tf_op jit(solution)/shard_map/all_gather | solution.py:89
  209.6 119.6 %all-gather.11.cloned.1.call-start = ((), (), s32[]{:S(2)}) async-start(), calls=%async_computation.7 | async-start | bytes 2621440 | tf_op jit(solution)/shard_map/all_gather | solution.py:90
Sparse Core Ops, SparseCore 0:
  16.8 77.8 reduce-scatter.4
  101.5 25.3 reduce-scatter.6
  130.4 43.5 all-reduce.1
  178.0 27.2 all-gather.4
  207.3 28.2 all-gather.6
  237.6 45.4 all-gather.8
  284.7 44.4 all-gather.10
where the time goes:
time: 344 us; the launch traced here: 340 us
  waiting for transfers between devices  245 us (71%)
  local copies, waits for them, and re-layouts  41.4 us (12%)
  matrix products  16.8 us (5%)
  between operations  16.2 us (5%)
  blocking collectives  12.8 us (4%)
  other arithmetic  7.46 us (2%)
    reduce_scatter x1, waiting for transfers between devices, body(): lax.psum_scatter(jnp.concatenate([contract_rows(input_act, query_cot), co...  78 us
    all_gather x1, waiting for transfers between devices, body(): lax.all_gather(new_out_w.astype(jnp.bfloat16), 'fs', axis=1, tiled=True)  42.1 us
    unnamed x26, local copies, waits for them, and re-layouts  41.4 us
    psum x1, waiting for transfers between devices, body(): lax.psum(projected.astype(jnp.bfloat16), 'rep').astype(jnp.float32)  39 us
    all_gather x1, waiting for transfers between devices, body(): lax.all_gather(new_query_w.astype(jnp.bfloat16), 'fs', axis=0, tiled=True)  26.8 us
    unnamed x8, waiting for transfers between devices  26.1 us
    all_gather x1, waiting for transfers between devices, body(): lax.all_gather(dir_o, 'fs', axis=0, tiled=True)  23.5 us
    psum x1, blocking collectives, body(): total_squares = lax.psum(local_squares, ('fs', 'tp'))  12.8 us
  transfers between devices with their start and end apart: 7, of which 7 were waited for; matrix products, arithmetic and copies ran while one was open for 12% of the time, Pallas kernels for 0%

commit v1 on v0

v1 whole, which is shorter than its diff:
```python
import functools
import math

import jax
import jax.numpy as jnp
from jax import lax
from jax.experimental import pallas as pl
from jax.experimental.pallas import tpu as pltpu
from jax.sharding import PartitionSpec as P

MESH = pl.DeviceIdType.MESH
F32 = jnp.float32
BF16 = jnp.bfloat16


def rcopy(src, dst, sems, index, there, **where):
    return pltpu.make_async_remote_copy(
        src_ref=src,
        dst_ref=dst,
        send_sem=sems[0].at[index],
        recv_sem=sems[1].at[there],
        device_id=where,
        device_id_type=MESH,
    )


def nt_dot(a, b):
    return lax.dot_general(a, b, (((1,), (1,)), ((), ())), preferred_element_type=F32)


def exchange_kernel(
    nf, nr, scale,
    x_ref, cq_ref, y_ref, ca_ref, wq_ref, wo_ref, fq_ref, fo_ref, m1q_ref, m2q_ref, m1o_ref, m2o_ref,
    fall_out, wq_out, wo_out, dir_out, proj_out, sq_out,
    acts, cots, cot_t, grads, fall, w32q, w32o, wbq, wbo, pieces, piece_in, summed, summed_in,
    moms, proj_all, dir_all, sq_buf,
    loc, fa_s, fa_r, fb_s, fb_r, fc_s, fc_r, wa_s, wa_r, wb_s, wb_r, ps_s, ps_r, ss_s, ss_r,
    pr_s, pr_r, da_s, da_r, db_s, db_r, sq_s, sq_r,
):
    f, r, t = lax.axis_index("fs"), lax.axis_index("rep"), lax.axis_index("tp")
    ot = 1 - t
    dl, rank = fq_ref.shape
    hl = cq_ref.shape[1]
    dq, hq = dl // nr, hl // nr
    rl = rank // nf
    pc = 2 * hl // nr
    ppa = nr // 2
    fa, fb, fc = (fa_s, fa_r), (fb_s, fb_r), (fc_s, fc_r)
    wa, wb = (wa_s, wa_r), (wb_s, wb_r)
    ps, ss, pr, da, db, sq = (ps_s, ps_r), (ss_s, ss_r), (pr_s, pr_r), (da_s, da_r), (db_s, db_r), (sq_s, sq_r)

    def fpeer(k):
        return lax.rem(f + k, nf)

    def rpeer(j):
        return lax.rem(r + j, nr)

    def each_f(body):
        lax.fori_loop(1, nf, lambda k, _: (body(k, fpeer(k)), 0)[1], 0)

    def rows(start, size):
        return pl.ds(pl.multiple_of(start, 16), size)

    def local(i, src, dst):
        return pltpu.make_async_copy(src, dst, loc.at[i])

    own_rows = rows(f * dl, dl)
    load_f = [local(0, fq_ref, fall.at[0, own_rows]), local(1, fo_ref, fall.at[1, own_rows])]
    load_w = [local(2, wq_ref, w32q), local(3, wo_ref, w32o)]
    load_c = [local(4, cq_ref, cots.at[0]), local(5, ca_ref, cots.at[1])]
    load_x = [local(6, x_ref, acts.at[0]), local(7, y_ref, acts.at[1])]
    for c in load_f + load_w + load_c + load_x:
        c.start()
    pcol = pl.ds(pl.multiple_of(lax.rem(r, ppa) * pc, pc), pc)

    @pl.when(r < ppa)
    def _():
        local(8, m1q_ref.at[:, pcol], moms.at[0]).start()
        local(9, m2q_ref.at[:, pcol], moms.at[1]).start()

    @pl.when(r >= ppa)
    def _():
        local(8, m1o_ref.at[:, pcol], moms.at[0]).start()
        local(9, m2o_ref.at[:, pcol], moms.at[1]).start()

    barrier = pltpu.get_barrier_semaphore()
    each_f(lambda k, p: pl.semaphore_signal(barrier, inc=1, device_id={"fs": p}, device_id_type=MESH))
    for j in range(1, nr):
        pl.semaphore_signal(barrier, inc=1, device_id={"rep": rpeer(j)}, device_id_type=MESH)
    pl.semaphore_signal(barrier, inc=1, device_id={"tp": ot}, device_id_type=MESH)
    pl.semaphore_wait(barrier, nf + nr - 1)

    def fchunk(core, block, part):
        ref = fall.at[core, rows(block * dl + part * dq, dq)]
        return ref

    def fa_copy(k, p):
        return rcopy(fchunk(t, f, r), fchunk(t, f, r), fa, p, f, fs=p)

    def fb_copy(p, j):
        return rcopy(fchunk(t, p, r), fchunk(t, p, r), fb, (p, rpeer(j)), (p, r), rep=rpeer(j))

    def fc_copy(p, part):
        return rcopy(fchunk(t, p, part), fchunk(t, p, part), fc, (p, part), (p, part), tp=ot)

    for c in load_f:
        c.wait()
    each_f(lambda k, p: fa_copy(k, p).start())

    for c in load_w:
        c.wait()
    wbq[...] = w32q[...].astype(BF16)
    wbo[...] = w32o[...].astype(BF16)
    keep_w = [local(2, wbq, wq_out.at[own_rows]), local(3, wbo, wo_out.at[f])]
    for c in keep_w:
        c.start()

    def wq_chunk(block):
        return wq_out.at[rows(block * dl + r * dq, dq)]

    def wo_chunk(block):
        return wo_out.at[block, rows(r * hq, hq)]

    def wa_copies(p):
        return (
            rcopy(wbq.at[rows(r * dq, dq)], wq_chunk(f), wa, (p, 0), (f, 0), fs=p),
            rcopy(wbo.at[rows(r * hq, hq)], wo_chunk(f), wa, (p, 1), (f, 1), fs=p),
        )

    def wa_recv(p):
        return (
            rcopy(wbq.at[rows(r * dq, dq)], wq_chunk(p), wa, (p, 0), (p, 0), fs=p),
            rcopy(wbo.at[rows(r * hq, hq)], wo_chunk(p), wa, (p, 1), (p, 1), fs=p),
        )

    def wb_copies(p, j):
        q = rpeer(j)
        return (
            rcopy(wq_chunk(p), wq_chunk(p), wb, (p, q, 0), (p, r, 0), rep=q),
            rcopy(wo_chunk(p), wo_chunk(p), wb, (p, q, 1), (p, r, 1), rep=q),
        )

    def wb_recv(p, j):
        q = rpeer(j)
        there_q = wq_out.at[rows(p * dl + q * dq, dq)]
        there_o = wo_out.at[p, rows(q * hq, hq)]
        return (
            rcopy(there_q, there_q, wb, (p, q, 0), (p, q, 0), rep=q),
            rcopy(there_o, there_o, wb, (p, q, 1), (p, q, 1), rep=q),
        )

    def start_all(copies):
        for c in copies:
            c.start()

    each_f(lambda k, p: start_all(wa_copies(p)))

    nb = min(512, x_ref.shape[1])

    def gradient(i):
        load_c[i].wait()
        cot_t[...] = cots[i].T
        load_x[i].wait()

        def column(n, _):
            cols = pl.ds(pl.multiple_of(n * nb, nb), nb)
            grads[i, :, cols] = jnp.dot(cot_t[...], acts[i, :, cols], preferred_element_type=F32).astype(BF16)
            return 0

        lax.fori_loop(0, x_ref.shape[1] // nb, column, 0)

    gradient(0)

    def forward_f(k, p):
        rcopy(fchunk(t, p, r), fchunk(t, p, r), fa, p, p, fs=p).wait_recv()
        for j in range(1, nr):
            fb_copy(p, j).start()
        fc_copy(p, r).start()

    each_f(forward_f)
    gradient(1)

    def across_f(k, p):
        for j in range(1, nr):
            q = rpeer(j)
            rcopy(fchunk(t, p, q), fchunk(t, p, q), fb, (p, q), (p, q), rep=q).wait_recv()
            fc_copy(p, q).start()

    each_f(across_f)

    def rest_f(k, p):
        for part in range(nr):
            rcopy(fchunk(ot, p, part), fchunk(ot, p, part), fc, (p, part), (p, part), tp=ot).wait_recv()

    each_f(rest_f)
    keep_f = local(0, fall, fall_out)
    keep_f.start()

    rb = min(256, rank)
    for i in range(2):
        def ranks(n, _, i=i):
            cols = pl.ds(pl.multiple_of(n * rb, rb), rb)
            term = jnp.dot(grads[i], fall[i, :, cols], preferred_element_type=F32).T.astype(BF16)
            for part in range(ppa):
                pieces[i * ppa + part, cols, :] = term[:, part * pc:(part + 1) * pc]
            return 0

        lax.fori_loop(0, rank // rb, ranks, 0)

    def ps_copy(j):
        q = rpeer(j)
        return rcopy(pieces.at[q], piece_in.at[r], ps, q, r, rep=q)

    for j in range(1, nr):
        ps_copy(j).start()

    def forward_w(k, p):
        for c in wa_recv(p):
            c.wait_recv()
        for j in range(1, nr):
            start_all(wb_copies(p, j))

    for j in range(1, nr):
        q = rpeer(j)
        rcopy(pieces.at[q], piece_in.at[q], ps, q, q, rep=q).wait_recv()
    total = pieces[r].astype(F32)
    for j in range(1, nr):
        total = total + piece_in[rpeer(j)].astype(F32)
    summed[...] = total.astype(BF16)

    def ss_copy(p):
        return rcopy(summed.at[rows(p * rl, rl)], summed_in.at[f], ss, p, f, fs=p)

    each_f(lambda k, p: ss_copy(p).start())
    each_f(forward_w)

    own_rank = rows(f * rl, rl)

    def gather_sum(k, total):
        p = fpeer(k)
        rcopy(summed.at[own_rank], summed_in.at[p], ss, p, p, fs=p).wait_recv()
        return total + summed_in[p].astype(F32)

    proj = lax.fori_loop(1, nf, gather_sum, summed[own_rank, :].astype(F32)).astype(BF16)
    proj_all[r] = proj

    def pr_copy(j):
        q = rpeer(j)
        return rcopy(proj_all.at[r], proj_all.at[r], pr, q, r, rep=q)

    proj = proj.astype(F32) * scale
    local(8, m1q_ref.at[:, pcol], moms.at[0]).wait()
    local(9, m2q_ref.at[:, pcol], moms.at[1]).wait()
    first = 0.8 * moms[0] + 0.2 * proj
    second = 0.9 * moms[1] + 0.1 * proj * proj
    dir_all[r, own_rank, :] = (first / jnp.sqrt(second)).astype(BF16)

    def da_copy(p):
        return rcopy(dir_all.at[r, own_rank], dir_all.at[r, own_rank], da, p, f, fs=p)

    each_f(lambda k, p: da_copy(p).start())
    for j in range(1, nr):
        pr_copy(j).start()

    def da_wait(k, p):
        there = dir_all.at[r, rows(p * rl, rl)]
        rcopy(there, there, da, p, p, fs=p).wait_recv()

    each_f(da_wait)

    def db_copy(j):
        q = rpeer(j)
        return rcopy(dir_all.at[r], dir_all.at[r], db, q, r, rep=q)

    for j in range(1, nr):
        db_copy(j).start()
    for j in range(1, nr):
        q = rpeer(j)
        rcopy(dir_all.at[q], dir_all.at[q], db, q, q, rep=q).wait_recv()
        rcopy(proj_all.at[q], proj_all.at[q], pr, q, q, rep=q).wait_recv()
    keep_d = [local(4, dir_all, dir_out), local(5, proj_all, proj_out)]
    start_all(keep_d)

    squares = jnp.zeros((8, pc), F32)
    for q in range(nr):
        d = dir_all[q].astype(F32)
        squares = squares + jnp.sum((d * d).reshape(rank // 8, 8, pc), axis=0)
    sq_buf[0] = squares
    sq_copy = rcopy(sq_buf.at[0], sq_buf.at[1], sq, 0, 0, tp=ot)
    sq_copy.start()
    sq_copy.wait_recv()
    sq_out[...] = jnp.zeros(sq_out.shape, F32) + jnp.sum(sq_buf[0] + sq_buf[1])

    def rest_w(k, p):
        for j in range(1, nr):
            for c in wb_recv(p, j):
                c.wait_recv()

    each_f(rest_w)

    def drain(k, p):
        fa_copy(k, p).wait_send()
        for c in wa_copies(p):
            c.wait_send()
        for j in range(1, nr):
            fb_copy(p, j).wait_send()
            for c in wb_copies(p, j):
                c.wait_send()
        for part in range(nr):
            fc_copy(p, part).wait_send()
        ss_copy(p).wait_send()
        da_copy(p).wait_send()

    each_f(drain)
    for j in range(1, nr):
        ps_copy(j).wait_send()
        pr_copy(j).wait_send()
        db_copy(j).wait_send()
    sq_copy.wait_send()
    for c in keep_w + [keep_f] + keep_d:
        c.wait()


def apply_kernel(
    nr, count, scale,
    fall_ref, wq_ref, wo_ref, dir_ref, proj_ref, sq_ref, w32q_ref, w32o_ref, fq_ref, fo_ref,
    m1q_ref, m2q_ref, m1o_ref, m2o_ref,
    nwq_ref, nwo_ref, sq_out, so_out, n1q_ref, n2q_ref, n1o_ref, n2o_ref, cq_ref, co_ref,
    dirs,
):
    ppa = nr // 2
    inverse = 1.0 / jnp.sqrt(sq_ref[0:1, 0:1] / count + 1e-06)

    @pl.when(pl.program_id(0) == 0)
    def _():
        dirs[0] = jnp.concatenate([dir_ref[q] for q in range(ppa)], axis=1)
        dirs[1] = jnp.concatenate([dir_ref[q] for q in range(ppa, nr)], axis=1).T
        step_q = jnp.dot(fq_ref[...], dirs[0], preferred_element_type=F32) * inverse
        sq_out[...] = step_q
        nwq_ref[...] = w32q_ref[...] - 0.01 * step_q
        step_o = nt_dot(dirs[1], fo_ref[...]) * inverse
        so_out[...] = step_o
        nwo_ref[...] = w32o_ref[...] - 0.01 * step_o
        proj_q = jnp.concatenate([proj_ref[q] for q in range(ppa)], axis=1).astype(F32) * scale
        proj_o = jnp.concatenate([proj_ref[q] for q in range(ppa, nr)], axis=1).astype(F32) * scale
        n1q_ref[...] = 0.8 * m1q_ref[...] + 0.2 * proj_q
        n2q_ref[...] = 0.9 * m2q_ref[...] + 0.1 * proj_q * proj_q
        n1o_ref[...] = 0.8 * m1o_ref[...] + 0.2 * proj_o
        n2o_ref[...] = 0.9 * m2o_ref[...] + 0.1 * proj_o * proj_o

    step_q = jnp.dot(fall_ref[0], dirs[0], preferred_element_type=F32) * inverse
    cq_ref[...] = (wq_ref[...].astype(F32) - 0.01 * step_q).astype(BF16)
    step_o = nt_dot(dirs[1], fall_ref[1]) * inverse
    whole_w = jnp.concatenate([wo_ref[m].astype(F32) for m in range(wo_ref.shape[0])], axis=1)
    co_ref[...] = (whole_w - 0.01 * step_o).astype(BF16)


def body(
    nf, nr,
    input_act, query_cot, out_cot, attn_out, query_w, out_w, query_factor, out_factor,
    first_q, second_q, first_o, second_o,
):
    tokens, d = input_act.shape
    hl = query_cot.shape[1]
    dl, rank = query_factor.shape
    rl = first_q.shape[0]
    pc = 2 * hl // nr
    scale = 1.0 / math.sqrt(tokens * nf * nr)
    anyspace = pl.BlockSpec(memory_space=pl.ANY)
    dma = pltpu.SemaphoreType.DMA
    sds = jax.ShapeDtypeStruct
    sems = []
    for shape in ((nf,), (nf, nr), (nf, nr), (nf, 2), (nf, nr, 2), (nr,), (nf,), (nr,), (nf,), (nr,), (1,)):
        sems += [dma(shape), dma(shape)]
    fall, wq_all, wo_all, dirs, projs, squares = pl.pallas_call(
        functools.partial(exchange_kernel, nf, nr, scale),
        out_shape=(
            sds((2, d, rank), BF16),
            sds((d, hl), BF16),
            sds((nf, hl, dl), BF16),
            sds((nr, rank, pc), BF16),
            sds((nr, rl, pc), BF16),
            sds((8, 128), F32),
        ),
        in_specs=[anyspace] * 12,
        out_specs=(anyspace,) * 5 + (pl.BlockSpec(memory_space=pltpu.VMEM),),
        scratch_shapes=[
            pltpu.VMEM((2, tokens, d), BF16),
            pltpu.VMEM((2, tokens, hl), BF16),
            pltpu.VMEM((hl, tokens), BF16),
            pltpu.VMEM((2, hl, d), BF16),
            pltpu.VMEM((2, d, rank), BF16),
            pltpu.VMEM((dl, hl), F32),
            pltpu.VMEM((hl, dl), F32),
            pltpu.VMEM((dl, hl), BF16),
            pltpu.VMEM((hl, dl), BF16),
            pltpu.VMEM((nr, rank, pc), BF16),
            pltpu.VMEM((nr, rank, pc), BF16),
            pltpu.VMEM((rank, pc), BF16),
            pltpu.VMEM((nf, rl, pc), BF16),
            pltpu.VMEM((2, rl, pc), F32),
            pltpu.VMEM((nr, rl, pc), BF16),
            pltpu.VMEM((nr, rank, pc), BF16),
            pltpu.VMEM((2, 8, pc), F32),
            dma((10,)),
        ] + sems,
        compiler_params=pltpu.CompilerParams(
            collective_id=0, has_side_effects=True, vmem_limit_bytes=48 * 1024 * 1024
        ),
    )(
        input_act, query_cot, out_cot, attn_out, query_w, out_w, query_factor, out_factor,
        first_q, second_q, first_o, second_o,
    )
    group = min(nf, max(1, 128 // dl))
    whole = lambda a: pl.BlockSpec(a.shape, lambda j, n=len(a.shape): (0,) * n)
    locals_in = (dirs, projs, squares, query_w, out_w, query_factor, out_factor, first_q, second_q, first_o, second_o)
    results = (query_w, out_w, query_w, out_w, first_q, second_q, first_o, second_o)
    outs = pl.pallas_call(
        functools.partial(apply_kernel, nr, 2 * rank * hl * 2, scale),
        grid=(nf // group,),
        out_shape=tuple(sds(a.shape, F32) for a in results) + (sds((d, hl), BF16), sds((hl, d), BF16)),
        in_specs=[
            pl.BlockSpec((2, group * dl, rank), lambda j: (0, j, 0)),
            pl.BlockSpec((group * dl, hl), lambda j: (j, 0)),
            pl.BlockSpec((group, hl, dl), lambda j: (j, 0, 0)),
        ] + [whole(a) for a in locals_in],
        out_specs=tuple(whole(a) for a in results) + (
            pl.BlockSpec((group * dl, hl), lambda j: (j, 0)),
            pl.BlockSpec((hl, group * dl), lambda j: (0, j)),
        ),
        scratch_shapes=[pltpu.VMEM((2, rank, hl), BF16)],
        compiler_params=pltpu.CompilerParams(vmem_limit_bytes=48 * 1024 * 1024),
    )(fall, wq_all, wo_all, *locals_in)
    return outs


def solution(mesh):
    return jax.shard_map(
        functools.partial(body, mesh.shape["fs"], mesh.shape["rep"]),
        mesh=mesh,
        in_specs=(
            P(("fs", "rep"), None),
            P(("fs", "rep"), "tp"),
            P(("fs", "rep"), None),
            P(("fs", "rep"), "tp"),
            P("fs", "tp"),
            P("tp", "fs"),
            P("fs", None),
            P("fs", None),
            P("fs", "tp"),
            P("fs", "tp"),
            P("fs", "tp"),
            P("fs", "tp"),
        ),
        out_specs=(
            P("fs", "tp"),
            P("tp", "fs"),
            P("fs", "tp"),
            P("tp", "fs"),
            P("fs", "tp"),
            P("fs", "tp"),
            P("fs", "tp"),
            P("fs", "tp"),
            P(None, "tp"),
            P("tp", None),
        ),
        check_vma=False,
    )
```

time: 344 us -> 136 us (0.40); the launches traced: 340 us -> 136 us
  waiting for transfers between devices: 245 us -> 0 us
  Pallas kernels: 0 us -> 126 us
  local copies, waits for them, and re-layouts: 41.4 us -> 9.39 us
  matrix products: 16.8 us -> 0 us
  between operations: 16.2 us -> 0.74 us
  blocking collectives: 12.8 us -> 0 us
  other arithmetic: 7.46 us -> 0 us
    pallas_call x0 -> x2, Pallas kernels: none -> 126 us  [the longest x1 117 us: body(): pl.pallas_call(functools.partial(exchange_kernel, nf, nr, scale), out_sha...]
    all_gather x4 -> x0, waiting for transfers between devices: 102 us -> none  [the longest x1 42.1 us: body(): lax.all_gather(new_out_w.astype(jnp.bfloat16), 'fs', axis=1, tiled=True)]
    reduce_scatter x1 -> x0, waiting for transfers between devices: 78 us -> none  [body(): lax.psum_scatter(jnp.concatenate([contract_rows(input_act, query_cot), co...]
    psum x1 -> x0, waiting for transfers between devices: 39 us -> none  [body(): lax.psum(projected.astype(jnp.bfloat16), 'rep').astype(jnp.float32)]
    unnamed x26 -> x30, local copies, waits for them, and re-layouts: 41.4 us -> 9.39 us
    unnamed x8 -> x0, waiting for transfers between devices: 26.1 us -> none
    dot_general x6 -> x0, matrix products: 16.8 us -> none  [the longest x2 8.54 us: exact_dot(): jnp.dot(left_side, right_side, precision=lax.Precision.HIGHEST, preferred...]
    psum x1 -> x0, blocking collectives: 12.8 us -> none  [body(): total_squares = lax.psum(local_squares, ('fs', 'tp'))]
  transfers between devices with their start and end apart: 7 -> 0, of which waited for: 7 -> 0; matrix products, arithmetic and copies ran while one was open for 12% -> 0% of each run, Pallas kernels for 0% -> 0%
where the time goes in v1:
time: 136 us
  Pallas kernels  126 us (93%)
  local copies, waits for them, and re-layouts  9.39 us (7%)
    pallas_call x1, Pallas kernels, body(): pl.pallas_call(functools.partial(exchange_kernel, nf, nr, scale), out_sha...  117 us
    unnamed x30, local copies, waits for them, and re-layouts  9.39 us
    pallas_call x1, Pallas kernels, body(): pl.pallas_call(functools.partial(apply_kernel, nr, 2 * rank * hl * 2, sca...  9.02 us

profile of v1, /device:TPU:9, one launch (start us, length us, event | category | flops | bytes accessed | tf_op | source)
XLA Modules:
  0.0 135.8 jit_solution(15585911187194319860)
XLA Ops:
  0.6 0.0 copy-start
  0.7 1.2 copy-done
  1.9 0.0 copy-start.3
  1.9 1.0 copy-done.3
  2.9 0.0 copy-start.5
  2.9 1.0 copy-done.5
  4.0 0.0 copy-start.7
  4.0 0.9 copy-done.7
  4.9 0.0 copy-start.9
  4.9 0.9 copy-done.9
  5.9 0.0 copy-start.11
  5.9 0.9 copy-done.11
  6.8 0.0 copy-start.12
  6.8 0.9 copy-done.12
  7.8 0.0 copy-start.13
  7.8 1.1 copy-done.13
  8.9 0.0 copy-start.14
  8.9 1.1 copy-done.14
  10.0 0.0 copy-start.1
  10.0 0.0 copy-start.2
  10.0 0.0 copy-start.4
  10.0 0.0 copy-start.6
  10.0 0.0 copy-start.8
  10.0 0.0 copy-start.10
  10.1 116.7 %shard_map.195 = (bf16[2,2048,512]{2,1,0:T(8,128)(2,1)}, bf16[2048,512]{1,0:T(8,128)(2,1)}, bf16[4,512,512]{2,1,0:T(8,128)(2,1)}, bf16[4,512,256]{2,1,0:T(8,128)...) custom-call(bf16[768,2048]{1,0:T(8,128)(2,1)} %x_ref.1, bf16[768,512]{1,0:T(8,128)(2,1)S(1)} %copy-done.13, ...), custom_call_target="tpu_custom_call" | custom-call | tf_op jit(solution)/shard_map/pallas_call | solution.py:375
  126.7 0.0 copy-done.1
  126.7 0.0 copy-done.2
  126.8 0.0 copy-done.4
  126.8 0.0 copy-done.6
  126.8 0.0 copy-done.8
  126.8 0.0 copy-done.10
  126.8 9.0 %shard_map.196 = (f32[512,512]{1,0:T(8,128)}, f32[512,512]{1,0:T(8,128)}, f32[512,512]{1,0:T(8,128)}, f32[512,512]{1,0:T(8,128)}, f32[128,512]{1,0:T(8,128)}, /*...) custom-call(bf16[2,2048,512]{2,1,0:T(8,128)(2,1)} %get-tuple-element, ...), custom_call_target="tpu_custom_call" | custom-call | tf_op jit(solution)/shard_map/pallas_call | solution.py:418
Async XLA Ops:
  0.6 1.2 copy-start
  1.9 1.0 copy-start.3
  2.9 1.0 copy-start.5
  4.0 0.9 copy-start.7
  4.9 0.9 copy-start.9
  5.9 0.9 copy-start.11
  6.8 0.9 copy-start.12
  7.8 1.1 copy-start.13
  8.9 1.1 copy-start.14
  10.0 116.7 %copy-start.1 = (f32[512,512]{1,0:T(8,128)S(1)}, f32[512,512]{1,0:T(8,128)}, u32[]{:S(2)}) copy-start(f32[512,512]{1,0:T(8,128)} %w32q_ref.1) | copy-start | bytes 3145732
  10.0 116.7 %copy-start.2 = (f32[512,512]{1,0:T(8,128)S(1)}, f32[512,512]{1,0:T(8,128)}, u32[]{:S(2)}) copy-start(f32[512,512]{1,0:T(8,128)} %w32o_ref.1) | copy-start | bytes 3145732
  10.0 116.7 %copy-start.4 = (bf16[512,512]{1,0:T(8,128)(2,1)S(1)}, bf16[512,512]{1,0:T(8,128)(2,1)}, u32[]{:S(2)}) copy-start(bf16[512,512]{1,0:T(8,128)(2,1)} %fq_ref.3) | copy-start | bytes 1572868
  10.0 116.7 %copy-start.6 = (bf16[512,512]{1,0:T(8,128)(2,1)S(1)}, bf16[512,512]{1,0:T(8,128)(2,1)}, u32[]{:S(2)}) copy-start(bf16[512,512]{1,0:T(8,128)(2,1)} %fo_ref.3) | copy-start | bytes 1572868
  10.0 116.7 %copy-start.8 = (f32[128,512]{1,0:T(8,128)S(1)}, f32[128,512]{1,0:T(8,128)}, u32[]{:S(2)}) copy-start(f32[128,512]{1,0:T(8,128)} %m1q_ref.3) | copy-start | bytes 786436
  10.0 116.7 %copy-start.10 = (f32[128,512]{1,0:T(8,128)S(1)}, f32[128,512]{1,0:T(8,128)}, u32[]{:S(2)}) copy-start(f32[128,512]{1,0:T(8,128)} %m2q_ref.3) | copy-start | bytes 786436

commit v2 on v1

--- a/solution.py
+++ b/solution.py
@@ -41,7 +41,8 @@
     ot = 1 - t
     dl, rank = fq_ref.shape
     hl = cq_ref.shape[1]
-    dq, hq = dl // nr, hl // nr
+    dq, hd = dl // nr, hl // 2
+    hq = (hl - hd) // nr
     rl = rank // nf
     pc = 2 * hl // nr
     ppa = nr // 2
@@ -55,8 +56,8 @@
     def rpeer(j):
         return lax.rem(r + j, nr)
 
-    def each_f(body):
-        lax.fori_loop(1, nf, lambda k, _: (body(k, fpeer(k)), 0)[1], 0)
+    def each_f(body, first=1, last=nf):
+        lax.fori_loop(first, last, lambda k, _: (body(k, fpeer(k)), 0)[1], 0)
 
     def rows(start, size):
         return pl.ds(pl.multiple_of(start, 16), size)
@@ -119,18 +120,24 @@
         return wq_out.at[rows(block * dl + r * dq, dq)]
 
     def wo_chunk(block):
-        return wo_out.at[block, rows(r * hq, hq)]
+        return wo_out.at[block, rows(hd + r * hq, hq)]
 
     def wa_copies(p):
         return (
             rcopy(wbq.at[rows(r * dq, dq)], wq_chunk(f), wa, (p, 0), (f, 0), fs=p),
-            rcopy(wbo.at[rows(r * hq, hq)], wo_chunk(f), wa, (p, 1), (f, 1), fs=p),
+            rcopy(wbo.at[rows(hd + r * hq, hq)], wo_chunk(f), wa, (p, 1), (f, 1), fs=p),
         )
+
+    def wd_copy(p):
+        return rcopy(wbo.at[pl.ds(0, hd)], wo_out.at[f, pl.ds(0, hd)], wa, (p, 2), (f, 2), fs=p)
+
+    def wd_recv(p):
+        return rcopy(wbo.at[pl.ds(0, hd)], wo_out.at[p, pl.ds(0, hd)], wa, (p, 2), (p, 2), fs=p)
 
     def wa_recv(p):
         return (
             rcopy(wbq.at[rows(r * dq, dq)], wq_chunk(p), wa, (p, 0), (p, 0), fs=p),
-            rcopy(wbo.at[rows(r * hq, hq)], wo_chunk(p), wa, (p, 1), (p, 1), fs=p),
+            rcopy(wbo.at[rows(hd + r * hq, hq)], wo_chunk(p), wa, (p, 1), (p, 1), fs=p),
         )
 
     def wb_copies(p, j):
@@ -143,7 +150,7 @@
     def wb_recv(p, j):
         q = rpeer(j)
         there_q = wq_out.at[rows(p * dl + q * dq, dq)]
-        there_o = wo_out.at[p, rows(q * hq, hq)]
+        there_o = wo_out.at[p, rows(hd + q * hq, hq)]
         return (
             rcopy(there_q, there_q, wb, (p, q, 0), (p, q, 0), rep=q),
             rcopy(there_o, there_o, wb, (p, q, 1), (p, q, 1), rep=q),
@@ -153,7 +160,9 @@
         for c in copies:
             c.start()
 
-    each_f(lambda k, p: start_all(wa_copies(p)))
+    each_f(lambda k, p: wa_copies(p)[0].start())
+    each_f(lambda k, p: wa_copies(p)[1].start())
+    each_f(lambda k, p: wd_copy(p).start())
 
     nb = min(512, x_ref.shape[1])
 
@@ -168,8 +177,6 @@
             return 0
 
         lax.fori_loop(0, x_ref.shape[1] // nb, column, 0)
-
-    gradient(0)
 
     def forward_f(k, p):
         rcopy(fchunk(t, p, r), fchunk(t, p, r), fa, p, p, fs=p).wait_recv()
@@ -177,7 +184,10 @@
             fb_copy(p, j).start()
         fc_copy(p, r).start()
 
-    each_f(forward_f)
+    early = 1 + (nf - 1) // 3
+    each_f(forward_f, 1, early)
+    gradient(0)
+    each_f(forward_f, early, nf)
     gradient(1)
 
     def across_f(k, p):
@@ -195,6 +205,16 @@
     each_f(rest_f)
     keep_f = local(0, fall, fall_out)
     keep_f.start()
+
+    def forward_w(which):
+        def step(k, p):
+            wa_recv(p)[which].wait_recv()
+            for j in range(1, nr):
+                wb_copies(p, j)[which].start()
+
+        each_f(step)
+
+    forward_w(0)
 
     rb = min(256, rank)
     for i in range(2):
@@ -214,12 +234,6 @@
     for j in range(1, nr):
         ps_copy(j).start()
 
-    def forward_w(k, p):
-        for c in wa_recv(p):
-            c.wait_recv()
-        for j in range(1, nr):
-            start_all(wb_copies(p, j))
-
     for j in range(1, nr):
         q = rpeer(j)
         rcopy(pieces.at[q], piece_in.at[q], ps, q, q, rep=q).wait_recv()
@@ -232,7 +246,7 @@
         return rcopy(summed.at[rows(p * rl, rl)], summed_in.at[f], ss, p, f, fs=p)
 
     each_f(lambda k, p: ss_copy(p).start())
-    each_f(forward_w)
+    forward_w(1)
 
     own_rank = rows(f * rl, rl)
 
@@ -292,6 +306,7 @@
     sq_out[...] = jnp.zeros(sq_out.shape, F32) + jnp.sum(sq_buf[0] + sq_buf[1])
 
     def rest_w(k, p):
+        wd_recv(p).wait_recv()
         for j in range(1, nr):
             for c in wb_recv(p, j):
                 c.wait_recv()
@@ -302,6 +317,7 @@
         fa_copy(k, p).wait_send()
         for c in wa_copies(p):
             c.wait_send()
+        wd_copy(p).wait_send()
         for j in range(1, nr):
             fb_copy(p, j).wait_send()
             for c in wb_copies(p, j):
@@ -366,11 +382,11 @@
     rl = first_q.shape[0]
     pc = 2 * hl // nr
     scale = 1.0 / math.sqrt(tokens * nf * nr)
-    anyspace = pl.BlockSpec(memory_space=pl.ANY)
+    anyspace = pl.BlockSpec(memory_space=pltpu.HBM)
     dma = pltpu.SemaphoreType.DMA
     sds = jax.ShapeDtypeStruct
     sems = []
-    for shape in ((nf,), (nf, nr), (nf, nr), (nf, 2), (nf, nr, 2), (nr,), (nf,), (nr,), (nf,), (nr,), (1,)):
+    for shape in ((nf,), (nf, nr), (nf, nr), (nf, 3), (nf, nr, 2), (nr,), (nf,), (nr,), (nf,), (nr,), (1,)):
         sems += [dma(shape), dma(shape)]
     fall, wq_all, wo_all, dirs, projs, squares = pl.pallas_call(
         functools.partial(exchange_kernel, nf, nr, scale),
@@ -405,7 +421,7 @@
             dma((10,)),
         ] + sems,
         compiler_params=pltpu.CompilerParams(
-            collective_id=0, has_side_effects=True, vmem_limit_bytes=48 * 1024 * 1024
+            collective_id=0, has_side_effects=True, vmem_limit_bytes=67043328
         ),
     )(
         input_act, query_cot, out_cot, attn_out, query_w, out_w, query_factor, out_factor,
@@ -429,7 +445,7 @@
             pl.BlockSpec((hl, group * dl), lambda j: (0, j)),
         ),
         scratch_shapes=[pltpu.VMEM((2, rank, hl), BF16)],
-        compiler_params=pltpu.CompilerParams(vmem_limit_bytes=48 * 1024 * 1024),
+        compiler_params=pltpu.CompilerParams(vmem_limit_bytes=67043328),
     )(fall, wq_all, wo_all, *locals_in)
     return outs
 

time: 136 us -> 111 us (0.82)
  Pallas kernels: 126 us -> 111 us
  local copies, waits for them, and re-layouts: 9.39 us -> 0 us
    pallas_call x1, Pallas kernels: 117 us -> 99.8 us  [body(): pl.pallas_call(functools.partial(exchange_kernel, nf, nr, scale), out_sha...]
    unnamed x30 -> x0, local copies, waits for them, and re-layouts: 9.39 us -> none
    pallas_call x1, Pallas kernels: 9.02 us -> 10.7 us  [body(): pl.pallas_call(functools.partial(apply_kernel, nr, 2 * rank * hl * 2, sca...]
where the time goes in v2:
time: 111 us
  Pallas kernels  111 us (100%)
    pallas_call x1, Pallas kernels, body(): pl.pallas_call(functools.partial(exchange_kernel, nf, nr, scale), out_sha...  99.8 us
    pallas_call x1, Pallas kernels, body(): pl.pallas_call(functools.partial(apply_kernel, nr, 2 * rank * hl * 2, sca...  10.7 us

profile of v2, /device:TPU:9, one launch (start us, length us, event | category | flops | bytes accessed | tf_op | source)
XLA Modules:
  0.0 111.2 jit_solution(3455188175658971500)
XLA Ops:
  0.6 99.8 %shard_map.195 = (bf16[2,2048,512]{2,1,0:T(8,128)(2,1)}, bf16[2048,512]{1,0:T(8,128)(2,1)}, bf16[4,512,512]{2,1,0:T(8,128)(2,1)}, bf16[4,512,256]{2,1,0:T(8,128)...) custom-call(bf16[768,2048]{1,0:T(8,128)(2,1)} %x_ref.1, bf16[768,512]{1,0:T(8,128)(2,1)} %cq_ref.1, ...), custom_call_target="tpu_custom_call" | custom-call | tf_op jit(solution)/shard_map/pallas_call | solution.py:391
  100.4 10.7 %shard_map.196 = (f32[512,512]{1,0:T(8,128)}, f32[512,512]{1,0:T(8,128)}, f32[512,512]{1,0:T(8,128)}, f32[512,512]{1,0:T(8,128)}, f32[128,512]{1,0:T(8,128)}, /*...) custom-call(bf16[2,2048,512]{2,1,0:T(8,128)(2,1)} %get-tuple-element, ...), custom_call_target="tpu_custom_call" | custom-call | tf_op jit(solution)/shard_map/pallas_call | solution.py:434
